TPU v7x, 32 devices: a whole 2x2x4 slice. The times are simulated.
32 devices in a mesh: sp: 16 (over z, y, x), tp: 2 (over core).
Axes of the slice: x: 2, y: 2, z: 4, core: 2. Of those that a mesh axis runs over, the one named last changes fastest.
Arguments:
- prompt: bfloat16 [1, 8192, 2048], P(None, 'sp', 'tp'), may hold values from -6 to 6
- new_token: bfloat16 [1, 2048], P(None, 'tp'), may hold values from -6 to 6
- w_query: bfloat16 [2048, 2048], P(None, 'tp'), may hold values from -0.125 to 0.125
- w_key: bfloat16 [2048, 2048], P(None, 'tp'), may hold values from -0.125 to 0.125
- w_value: bfloat16 [2048, 2048], P(None, 'tp'), may hold values from -0.125 to 0.125
- decay_rate: float32 [16], P('tp'), may hold values from 1e-05 to 0.06
- norm_gain: float32 [2048], P('tp'), may hold values from 0.1 to 1.9
Outputs:
- mixed: bfloat16 [1, 8192, 2048], P(None, 'sp', 'tp')
- cache: bfloat16 [1, 16, 128, 128], P(None, 'tp', 'sp')
- new_read: bfloat16 [1, 2048], P(None, 'tp')
All inputs are finite; a program needn't handle non-finite values.
Results may differ from a plain program's by a relative error of at most 0.0083.
Values may be sent and summed in bfloat16 or wider, within the bound.
A program may use at most 64 MiB of HBM per device.

v0:
```python
import jax
import jax.numpy as jnp
from jax import lax
from jax.sharding import PartitionSpec as P

HEAD = 128


rope_base = 10000.0
norm_floor = 1e-05


def rotate(tensor, positions):
    head_width = tensor.shape[-1]
    inverse = rope_base ** (-jnp.arange(0, head_width, 2, dtype=jnp.float32) / head_width)
    angles = positions.astype(jnp.float32)[:, None] * inverse[None, :]
    cosine = jnp.cos(angles)[:, None, :]
    sine_part = jnp.sin(angles)[:, None, :]
    first_half = tensor[..., : head_width // 2]
    second_half = tensor[..., head_width // 2 :]
    return jnp.concatenate(
        [
            first_half * cosine - second_half * sine_part,
            first_half * sine_part + second_half * cosine,
        ],
        axis=-1,
    )


def head_norm(output, gain):
    center = jnp.mean(output, axis=-1, keepdims=True)
    spread = jnp.mean(jnp.square(output - center), axis=-1, keepdims=True)
    return (output - center) * lax.rsqrt(spread + norm_floor) * gain


def decay_tables(log_gamma, block_size):
    offsets = jnp.arange(block_size, dtype=jnp.float32)
    gap_table = offsets[:, None] - offsets[None, :]
    within = jnp.where(
        gap_table[None] >= 0,
        jnp.exp(jnp.maximum(gap_table, 0.0)[None] * log_gamma[:, None, None]),
        0.0,
    )
    query_decay = jnp.exp((offsets[:, None] + 1.0) * log_gamma[None, :])
    key_decay = jnp.exp((block_size - 1.0 - offsets[:, None]) * log_gamma[None, :])
    return (within, query_decay, key_decay)


def per_device(prompt, new_token, w_query, w_key, w_value, decay_rate, norm_gain):
    sequences, block_size, feature_part = prompt.shape
    head_count = w_query.shape[1] // HEAD
    members = lax.axis_size("sp")
    device_rank = lax.axis_index("sp")
    prompt_rows = sequences * block_size
    token_rows = jnp.concatenate([prompt.reshape(prompt_rows, feature_part), new_token], axis=0)
    weight_list = (w_query, w_key, w_value)
    shard_piece = lax.all_gather(token_rows, "tp", axis=1, tiled=True)
    projected = tuple(
        (jnp.dot(shard_piece, weight, preferred_element_type=jnp.float32) for weight in weight_list)
    )
    full_shape = (sequences, block_size, head_count, HEAD)
    queries, key_rows, values = [
        tensor[:prompt_rows].astype(jnp.bfloat16).reshape(full_shape) for tensor in projected
    ]
    token_query, token_key, token_value = [
        tensor[prompt_rows:].astype(jnp.bfloat16).reshape(sequences, 1, head_count, HEAD)
        for tensor in projected
    ]
    positions = device_rank * block_size + jnp.arange(block_size, dtype=jnp.int32)
    scaled = (rotate(queries.astype(jnp.float32), positions) * HEAD ** (-0.5)).astype(jnp.bfloat16)
    turned = rotate(key_rows.astype(jnp.float32), positions).astype(jnp.bfloat16)
    log_gamma = -decay_rate
    within, query_decay, key_decay = decay_tables(log_gamma, block_size)
    weighted = (turned.astype(jnp.float32) * key_decay[None, :, :, None]).astype(jnp.bfloat16)
    local_state = jnp.einsum(
        "smhd,smhe->shde", weighted, values, preferred_element_type=jnp.float32
    )
    pieces = lax.all_to_all(local_state[None], "sp", split_axis=3, concat_axis=0, tiled=True)
    source_index = jnp.arange(members, dtype=jnp.float32)
    gap_table = source_index[:, None] - 1.0 - source_index[None, :]
    weights = jnp.where(
        gap_table[None] >= 0,
        jnp.exp(jnp.maximum(gap_table, 0.0)[None] * block_size * log_gamma[:, None, None]),
        0.0,
    )
    prefix = jnp.einsum("hji,ishre->jshre", weights, pieces, precision=lax.Precision.HIGHEST)
    tail_all = jnp.exp((members - 1.0 - source_index)[None, :] * block_size * log_gamma[:, None])
    final_rows = jnp.einsum("hi,ishre->shre", tail_all, pieces, precision=lax.Precision.HIGHEST)
    incoming = lax.all_to_all(
        prefix.astype(jnp.bfloat16), "sp", split_axis=0, concat_axis=3, tiled=True
    ).astype(prefix.dtype)[0]
    scores = (
        jnp.einsum("snhd,smhd->shnm", scaled, turned, preferred_element_type=jnp.float32)
        * within[None]
    )
    inner_part = jnp.einsum(
        "shnm,smhe->snhe", scores.astype(jnp.bfloat16), values, preferred_element_type=jnp.float32
    )
    carried = (
        jnp.einsum(
            "snhd,shde->snhe",
            scaled,
            incoming.astype(jnp.bfloat16),
            preferred_element_type=jnp.float32,
        )
        * query_decay[None, :, :, None]
    )
    gain = norm_gain.reshape(head_count, HEAD)
    mixed = (
        head_norm(inner_part + carried, gain)
        .astype(jnp.bfloat16)
        .reshape(sequences, block_size, head_count * HEAD)
    )
    cache = final_rows.astype(jnp.bfloat16)
    token_positions = jnp.full((1,), block_size * members, jnp.int32)
    token_scaled = (
        rotate(token_query.astype(jnp.float32), token_positions) * HEAD ** (-0.5)
    ).astype(jnp.bfloat16)[:, 0]
    token_turned = rotate(token_key.astype(jnp.float32), token_positions).astype(jnp.bfloat16)[:, 0]
    row_count = final_rows.shape[2]
    query_rows = lax.dynamic_slice_in_dim(
        token_scaled, device_rank * row_count, row_count, 2
    ).astype(jnp.float32)
    partial_value = jnp.einsum(
        "shr,shre->she", query_rows, final_rows, precision=lax.Precision.HIGHEST
    )
    read_sum = lax.psum(partial_value, "sp")
    own_score = jnp.sum(
        token_scaled.astype(jnp.float32) * token_turned.astype(jnp.float32), axis=-1, keepdims=True
    )
    read_out = jnp.exp(log_gamma)[None, :, None] * read_sum + own_score * token_value[:, 0].astype(
        jnp.float32
    )
    new_read = head_norm(read_out, gain).astype(jnp.bfloat16).reshape(sequences, head_count * HEAD)
    return (mixed, cache, new_read)


def solution(mesh):
    in_specs = (
        P(None, "sp", "tp"),
        P(None, "tp"),
        P(None, "tp"),
        P(None, "tp"),
        P(None, "tp"),
        P("tp"),
        P("tp"),
    )
    out_specs = (P(None, "sp", "tp"), P(None, "tp", "sp", None), P(None, "tp"))
    return jax.shard_map(
        per_device, mesh=mesh, in_specs=in_specs, out_specs=out_specs, check_vma=False
    )
```

profile of v0, /device:TPU:0, one launch (start us, length us, event | category | flops | bytes accessed | tf_op | source)
XLA Modules:
  0.0 131.3 jit_solution(5846563984525811698)
XLA Ops:
  7.2 0.0 all-gather.2.cloned.1.call-start
  7.2 2.3 %pad_maximum_fusion = bf16[513,1024]{1,0:T(8,128)(2,1)} fusion(bf16[1,1024]{1,0:T(2,128)(2,1)} %param.8, bf16[512,1024]{1,0:T(8,128)(2,1)} %bitcast.117), kind=kLoop, calls=%fused_computation.26 | loop fusion | flops 2101248 | bytes 2101248 | tf_op jit(solution)/shard_map/concatenate | solution.py:55
  9.6 0.1 multiply_sine_fusion.1
  9.7 0.3 fusion.16
  10.0 1.2 fusion.15
  11.1 0.1 fusion.34
  11.2 0.1 multiply_exponential_fusion.2
  11.3 0.1 maximum_multiply_fusion.1
  11.3 0.1 multiply_exponential_fusion.1
  11.4 1.0 multiply_cosine_fusion
  12.4 10.7 %all-gather.2.cloned.1.call-done = bf16[513,2048]{1,0:T(8,128)(2,1)} async-done(((bf16[513,1024]{1,0:T(8,128)(2,1)}), bf16[513,2048]{1,0:T(8,128)(2,1)}) %all-gather.2.cloned.1.call-update) | async-done | bytes 2101264 | tf_op jit(solution)/shard_map/all_gather | solution.py:57
  23.1 5.3 %convolution_convert_fusion = bf16[513,1024]{1,0:T(8,128)(2,1)S(1)} fusion(bf16[513,2048]{1,0:T(8,128)(2,1)} %all-gather.2.cloned.1.call-done, bf16[2048,1024]{1,0:T(8,128)(2,1)} %param.10), kind=kOutput, calls=%fused_computation.20 | convolution fusion | flops 2152203264 | bytes 7346176 | tf_op jit(solution)/shard_map/dot_general | solution.py:59
  28.5 0.2 convert_bitcast_fusion
  28.7 1.3 %copy-done.7 = bf16[513,2048]{1,0:T(8,128)(2,1)S(1)} copy-done((bf16[513,2048]{1,0:T(8,128)(2,1)S(1)}, bf16[513,2048]{1,0:T(8,128)(2,1)}, u32[]{:S(2)}) %copy-start.7) | copy-done | bytes 2101272
  30.0 2.4 %convolution_convert_fusion.1 = bf16[513,1024]{1,0:T(8,128)(2,1)S(1)} fusion(bf16[513,2048]{1,0:T(8,128)(2,1)S(1)} %copy-done.7, bf16[2048,1024]{1,0:T(8,128)(2,1)S(1)} %copy-done.5), kind=kOutput, calls=%fused_computation.21 | convolution fusion | flops 2152203264 | bytes 7346176 | tf_op jit(solution)/shard_map/dot_general | solution.py:59
  32.5 0.2 convert_bitcast_fusion.1
  32.7 0.5 copy.71
  33.2 0.5 copy.70
  33.7 1.3 %fusion.49 = (f32[1,512,8,64]{3,2,1,0:T(8,128)S(1)}, f32[1,512,8,64]{3,2,1,0:T(8,128)S(1)}, f32[1,512,8,64]{3,2,1,0:T(8,128)S(1)}, f32[1,512,8,64]{3,2,1,0:T(8,128)S(1)}) fusion(f32[1,512,8,128]{3,2,1,0:T(8,128)S(1)} %bitcast.112, f32[1,512,8,128]{3,2,1,0:T(8,128)S(1)} %bitcast.113), kind=kLoop, calls=%fused_computation.104 | loop fusion | bytes 8388608 | tf_op jit(solution)/shard_map/slice | solution.py:19
  35.0 2.8 %fusion.10 = (bf16[512,8,64]{2,0,1:T(8,128)(2,1)S(1)}, bf16[512,8,64]{2,0,1:T(8,128)(2,1)S(1)}, f32[512,8,64]{2,0,1:T(8,128)S(1)}, f32[512,8,64]{2,0,1:T(8,128)}) fusion(f32[1,512,8,64]{3,2,1,0:T(8,128)S(1)} %get-tuple-element.22, f32[1,512,8,64]{3,2,1,0:T(8,128)S(1)} %get-tuple-element.21, f32[512,64]{1,0:T(8,128)S(1)} %get-tuple-element.32, ...), kind=kLoop, calls=%fused_computation.27 | loop fusion | flops 3670016 | bytes 7602176 | tf_op jit(solution)/shard_map/concatenate | solution.py:21
  37.9 2.4 %convolution_convert_fusion.2 = bf16[513,1024]{1,0:T(8,128)(2,1)S(1)} fusion(bf16[513,2048]{1,0:T(8,128)(2,1)S(1)} %copy-done.7, bf16[2048,1024]{1,0:T(8,128)(2,1)S(1)} %copy-done.6), kind=kOutput, calls=%fused_computation.22 | convolution fusion | flops 2152203264 | bytes 7346176 | tf_op jit(solution)/shard_map/dot_general | solution.py:59
  40.3 2.6 %convolution_bitcast_fusion = f32[1,1,8,128,128]{4,3,2,1,0:T(8,128)S(1)} fusion(f32[512,8]{0,1:T(8,128)S(1)} %get-tuple-element.37, bf16[512,8,64]{2,0,1:T(8,128)(2,1)S(1)} %get-tuple-element.18, bf16[512,8,64]{2,0,1:T(8,128)(2,1)S(1)} %get-tuple-element.17, bf16[513,1024]{1,0:T(8,128)(2,1)S(1)} %convolution_convert_fusion.2), kind=kOutput, calls=%fused_computation.23 | convolution fusion | flops 137363456 | bytes 3686400 | tf_op jit(solution)/shard_map/smhd,smhe->shde/dot_general | solution.py:75
  43.0 1.1 copy.49
  44.1 6.8 %all-to-all-start = ((f32[1,1,8,128,128]{4,2,1,0,3:T(8,128)}), f32[1,1,8,128,128]{4,2,1,0,3:T(8,128)S(1)}, u32[]{:S(2)}, u32[]{:S(2)}) async-start(f32[1,1,8,128,128]{4,2,1,0,3:T(8,128)} %copy.49), calls=%async_computation | async-start | bytes 1048576 | tf_op jit(solution)/shard_map/all_to_all | solution.py:78
  50.9 0.1 fusion.40
  51.0 0.1 fusion.35
  51.0 0.1 dynamic-slice_bitcast_fusion
  51.1 0.2 multiply_reduce_fusion.2
  51.3 3.2 %fusion.7 = bf16[512,8,128]{2,0,1:T(8,128)(2,1)} fusion(f32[512,8,64]{2,0,1:T(8,128)S(1)} %get-tuple-element.25, f32[512,8,64]{2,0,1:T(8,128)} %get-tuple-element.26), kind=kLoop, calls=%fused_computation.8 | loop fusion | flops 1572864 | bytes 3145728 | tf_op jit(solution)/shard_map/convert_element_type | solution.py:70
  54.5 0.7 slice_convert_fusion
  55.2 7.4 %fusion = f32[8,128,512]{2,1,0:T(8,128)} fusion(f32[8]{0:T(128)S(1)} %get-tuple-element.36, f32[512,512]{1,0:T(8,128)} %fusion.15, pred[512,512]{1,0:T(8,128)(4,1)S(1)} %fusion.16, bf16[512,8,128]{2,0,1:T(8,128)(2,1)} %fusion.7, bf16[512,8,64]{2,0,1:T(8,128)(2,1)} %copy-done.2, bf16[512,8,64]{2,0,1:T(8,128)(2,1)} %copy-done.1, bf16[513,1024]{1,0:T(8,128)(2,1)} %copy-done.4), kind=kOutput, calls=%fused_computation.1 | convolution fusion | flops 1084227584 | bytes 7602208 | tf_op jit(solution)/shard_map/shnm,smhe->snhe/dot_general | solution.py:96
  62.6 3.8 %all-to-all-done = f32[1,1,8,128,128]{4,2,1,0,3:T(8,128)S(1)} async-done(((f32[1,1,8,128,128]{4,2,1,0,3:T(8,128)}), f32[1,1,8,128,128]{4,2,1,0,3:T(8,128)S(1)}, u32[]{:S(2)}, u32[]{:S(2)}) %all-to-all-start) | async-done | bytes 524320 | tf_op jit(solution)/shard_map/all_to_all | solution.py:78
  66.4 0.7 fusion.19
  67.1 0.9 fusion.9
  68.0 0.8 copy.52
  68.7 0.1 fusion.38
  68.9 39.2 %psum.7 = f32[1,8,128]{2,1,0:T(8,128)S(1)} all-reduce(f32[1,8,128]{2,1,0:T(8,128)S(1)} %bitcast.127), channel_id=1, replica_groups=mesh['sp'=16,'tp'=2] {'sp'}, use_global_device_ids=true, to_apply=%region_2.3 | all-reduce | flops 1024 | bytes 8192 | tf_op jit(solution)/shard_map/psum | solution.py:127
  108.1 0.2 fusion.48
  108.3 3.5 %all-to-all-start.1 = ((bf16[16,1,8,8,128]{4,3,2,1,0:T(8,128)(2,1)}), bf16[16,1,8,8,128]{4,3,2,1,0:T(8,128)(2,1)S(1)}, u32[]{:S(2)}, u32[]{:S(2)}) async-start(bf16[16,1,8,8,128]{4,3,2,1,0:T(8,128)(2,1)} %copy.52), calls=%async_computation.1 | async-start | bytes 524288 | tf_op jit(solution)/shard_map/all_to_all | solution.py:89
  111.8 0.2 multiply_reduce_fusion.1
  112.0 0.1 fusion.42
  112.1 0.6 copy.114
  112.7 0.6 convert_bitcast_fusion.2
  113.3 7.0 %all-to-all-done.1 = bf16[16,1,8,8,128]{4,3,2,1,0:T(8,128)(2,1)S(1)} async-done(((bf16[16,1,8,8,128]{4,3,2,1,0:T(8,128)(2,1)}), bf16[16,1,8,8,128]{4,3,2,1,0:T(8,128)(2,1)S(1)}, u32[]{:S(2)}, u32[]{:S(2)}) %all-to-all-start.1) | async-done | bytes 262176 | tf_op jit(solution)/shard_map/all_to_all | solution.py:89
  120.3 2.1 %fusion.51 = (f32[512,8]{0,1:T(8,128)S(1)}, f32[1,512,8,128]{1,3,2,0:T(8,128)S(1)}) fusion(f32[512,8]{0,1:T(8,128)S(1)} %get-tuple-element.38, bf16[512,8,128]{2,0,1:T(8,128)(2,1)S(1)} %copy-done, bf16[16,1,8,8,128]{4,3,2,1,0:T(8,128)(2,1)S(1)} %all-to-all-done.1, f32[8,128,512]{2,1,0:T(8,128)} %fusion), kind=kOutput, calls=%fused_computation.106 | convolution fusion | flops 135786496 | bytes 5537792 | tf_op jit(solution)/shard_map/snhd,shde->snhe/dot_general | solution.py:100
  122.4 0.3 multiply_reduce_fusion
  122.8 0.4 multiply_convert_fusion.2
  123.1 1.3 %copy.55 = bf16[1,512,1024]{2,1,0:T(8,128)(2,1)} copy(bf16[1,512,1024]{1,2,0:T(8,128)(2,1)S(1)} %bitcast.116) | data formatting | bytes 2097152
  (30 shorter events, 0.1 us)
Async XLA Ops:
  7.2 15.9 %all-gather.2.cloned.1.call-start = ((), (), s32[]{:S(2)}) async-start(), calls=%async_computation.2 | async-start | bytes 3194880 | tf_op jit(solution)/shard_map/all_gather | solution.py:57
  7.2 3.9 %copy-start.8 = (f32[8]{0:T(128)S(1)}, f32[8]{0:T(128)}, u32[]{:S(2)}) copy-start(f32[8]{0:T(128)} %param.12) | copy-start | bytes 100
  23.1 5.6 %copy-start.5 = (bf16[2048,1024]{1,0:T(8,128)(2,1)S(1)}, bf16[2048,1024]{1,0:T(8,128)(2,1)}, u32[]{:S(2)}) copy-start(bf16[2048,1024]{1,0:T(8,128)(2,1)} %param.9) | copy-start | bytes 12582916
  28.4 1.6 %copy-start.7 = (bf16[513,2048]{1,0:T(8,128)(2,1)S(1)}, bf16[513,2048]{1,0:T(8,128)(2,1)}, u32[]{:S(2)}) copy-start(bf16[513,2048]{1,0:T(8,128)(2,1)} %all-gather.2.cloned.1.call-done) | copy-start | bytes 6303748
  35.0 2.8 %copy-start.6 = (bf16[2048,1024]{1,0:T(8,128)(2,1)S(1)}, bf16[2048,1024]{1,0:T(8,128)(2,1)}, u32[]{:S(2)}) copy-start(bf16[2048,1024]{1,0:T(8,128)(2,1)} %param.11) | copy-start | bytes 12582916
  37.9 2.4 %copy-start.1 = (bf16[512,8,64]{2,0,1:T(8,128)(2,1)}, bf16[512,8,64]{2,0,1:T(8,128)(2,1)S(1)}, u32[]{:S(2)}) copy-start(bf16[512,8,64]{2,0,1:T(8,128)(2,1)S(1)} %get-tuple-element.17) | copy-start | bytes 1572868
  37.9 2.4 %copy-start.2 = (bf16[512,8,64]{2,0,1:T(8,128)(2,1)}, bf16[512,8,64]{2,0,1:T(8,128)(2,1)S(1)}, u32[]{:S(2)}) copy-start(bf16[512,8,64]{2,0,1:T(8,128)(2,1)S(1)} %get-tuple-element.18) | copy-start | bytes 1572868
  40.3 2.7 %copy-start.4 = (bf16[513,1024]{1,0:T(8,128)(2,1)}, bf16[513,1024]{1,0:T(8,128)(2,1)S(1)}, u32[]{:S(2)}) copy-start(bf16[513,1024]{1,0:T(8,128)(2,1)S(1)} %convolution_convert_fusion.2) | copy-start | bytes 3151876
  44.1 22.3 %all-to-all-start = ((f32[1,1,8,128,128]{4,2,1,0,3:T(8,128)}), f32[1,1,8,128,128]{4,2,1,0,3:T(8,128)S(1)}, u32[]{:S(2)}, u32[]{:S(2)}) async-start(f32[1,1,8,128,128]{4,2,1,0,3:T(8,128)} %copy.49), calls=%async_computation | async-start | bytes 1048576 | tf_op jit(solution)/shard_map/all_to_all | solution.py:78
  62.6 49.4 %copy-start.3 = (f32[1024]{0:T(1024)S(1)}, f32[1024]{0:T(1024)}, u32[]{:S(2)}) copy-start(f32[1024]{0:T(1024)} %param.13) | copy-start | bytes 12292
  62.6 57.7 %copy-start = (bf16[512,8,128]{2,0,1:T(8,128)(2,1)S(1)}, bf16[512,8,128]{2,0,1:T(8,128)(2,1)}, u32[]{:S(2)}) copy-start(bf16[512,8,128]{2,0,1:T(8,128)(2,1)} %fusion.7) | copy-start | bytes 3145732
  108.3 12.0 %all-to-all-start.1 = ((bf16[16,1,8,8,128]{4,3,2,1,0:T(8,128)(2,1)}), bf16[16,1,8,8,128]{4,3,2,1,0:T(8,128)(2,1)S(1)}, u32[]{:S(2)}, u32[]{:S(2)}) async-start(bf16[16,1,8,8,128]{4,3,2,1,0:T(8,128)(2,1)} %copy.52), calls=%async_computation.1 | async-start | bytes 524288 | tf_op jit(solution)/shard_map/all_to_all | solution.py:89
Sparse Core Ops, SparseCore 0:
  9.7 13.3 all-gather.1
where the time goes:
time: 132 us; the launch traced here: 131 us
  blocking collectives  39.2 us (30%)
  matrix products  24.1 us (18%)
  waiting for transfers between devices  21.4 us (16%)
  other arithmetic  14.4 us (11%)
  between operations  14.3 us (11%)
  starting transfers between devices  10.4 us (8%)
  local copies, waits for them, and re-layouts  7.52 us (6%)
    psum x1, blocking collectives, per_device(): read_sum = lax.psum(partial_value, 'sp')  39.2 us
    all_gather x1, waiting for transfers between devices, per_device(): shard_piece = lax.all_gather(token_rows, 'tp', axis=1, tiled=True)  10.7 us
    dot_general x3, matrix products, per_device(): jnp.dot(shard_piece, weight, preferred_element_type=jnp.float32)  10.2 us
    dot_general x1, matrix products, per_device(): jnp.einsum('shnm,smhe->snhe', scores.astype(jnp.bfloat16), values, prefer...  7.39 us
    all_to_all x1, waiting for transfers between devices, per_device(): lax.all_to_all(prefix.astype(jnp.bfloat16), 'sp', split_axis=0, concat_ax...  6.98 us
    all_to_all x1, starting transfers between devices, per_device(): lax.all_to_all(local_state[None], 'sp', split_axis=3, concat_axis=0, tile...  6.79 us
    unnamed x22, local copies, waits for them, and re-layouts  4.22 us
    all_to_all x1, waiting for transfers between devices, per_device(): lax.all_to_all(local_state[None], 'sp', split_axis=3, concat_axis=0, tile...  3.77 us
  transfers between devices with their start and end apart: 3, of which 3 were waited for; matrix products, arithmetic and copies ran while one was open for 12% of the time, Pallas kernels for 0%

commit v1 on v0

v1 whole, which is shorter than its diff:
```python
import functools

import jax
import jax.numpy as jnp
import numpy as np
from jax import lax
from jax.experimental import pallas as pl
from jax.experimental.pallas import tpu as pltpu
from jax.sharding import PartitionSpec as P

HEAD = 128
PAD = 16
rope_base = 10000.0
norm_floor = 1e-05
MESH = pl.DeviceIdType.MESH
BF = jnp.bfloat16
F32 = jnp.float32


def head_norm(o, gain):
    center = jnp.mean(o, axis=-1, keepdims=True)
    delta = o - center
    spread = jnp.mean(delta * delta, axis=-1, keepdims=True)
    return delta * lax.rsqrt(spread + norm_floor) * gain


def split(members):
    best = 1
    for g in range(1, members + 1):
        if members % g == 0 and g * g <= members:
            best = g
    return best


def dot(a, b):
    return jnp.dot(a, b, preferred_element_type=F32)


def kernel(cfg, x_hbm, tok_hbm, wq, wk, wv, rate, gain, tab_hbm, base, mixed, cache, read_out,
           xbuf, tokbuf, wbuf, acc, tab, ctab, stab, kbuf, qbuf, vbuf, intra, obuf,
           send1, recv1, pre, recv2, send3, recv3, pacc, fin, tokq, tokk, tokv, rdbuf,
           w_sem, l_sem, tps, tpr, s1s, s1r, s2s, s2r, s3s, s3r, rds, rdr, o_sem):
    M, G, Z, T, B, F, H, hc, R = cfg
    NC = H // hc
    W = hc * HEAD
    rank = lax.axis_index("sp")
    me = lax.axis_index("tp")
    z = rank // G
    j = rank % G
    weights = (wk, wv, wq)

    lx = pltpu.make_async_copy(x_hbm, xbuf.at[me, pl.ds(0, B)], l_sem.at[0])
    lt = pltpu.make_async_copy(tok_hbm, tokbuf.at[me], l_sem.at[1])
    ltab = pltpu.make_async_copy(tab_hbm, tab, l_sem.at[2])
    lx.start()
    lt.start()

    def wcopy(m, c, d):
        p = lax.rem(me + d, T)
        return pltpu.make_async_copy(
            weights[m].at[pl.ds(pl.multiple_of(p * F, HEAD), F), pl.ds(c * W, W)],
            wbuf.at[m, c, d], w_sem.at[m, c, d])

    for c in range(NC):
        wcopy(0, c, 0).start()
        wcopy(1, c, 0).start()
        if c == 0:
            ltab.start()
    for c in range(NC):
        for d in range(1, T):
            wcopy(0, c, d).start()
            wcopy(1, c, d).start()
    for c in range(NC):
        for d in range(T):
            wcopy(2, c, d).start()

    barrier = pltpu.get_barrier_semaphore()
    for d in range(1, T):
        pl.semaphore_signal(barrier, inc=1, device_id={"tp": lax.rem(me + d, T)}, device_id_type=MESH)
    for d in range(1, M):
        pl.semaphore_signal(barrier, inc=1, device_id={"sp": lax.rem(rank + d, M)}, device_id_type=MESH)

    def widen(p):
        t = tokbuf[p].astype(F32)
        xbuf[p, B:B + PAD, :] = jnp.broadcast_to(t, (PAD, F)).astype(BF)

    lt.wait()
    widen(me)
    lx.wait()

    def own_part(c):
        for m in range(2):
            wcopy(m, c, 0).wait()
            acc[m, c] = dot(xbuf[me], wbuf[m, c, 0])

    own_part(0)
    pl.semaphore_wait(barrier, T - 1 + M - 1)
    sends = []
    for d in range(1, T):
        peer = lax.rem(me + d, T)
        a = pltpu.make_async_remote_copy(
            src_ref=x_hbm, dst_ref=xbuf.at[me, pl.ds(0, B)], send_sem=tps.at[0, d],
            recv_sem=tpr.at[0, d], device_id={"tp": peer}, device_id_type=MESH)
        b = pltpu.make_async_remote_copy(
            src_ref=tok_hbm, dst_ref=tokbuf.at[me], send_sem=tps.at[1, d],
            recv_sem=tpr.at[1, d], device_id={"tp": peer}, device_id_type=MESH)
        a.start()
        b.start()
        sends += [a, b]

    ltab.wait()
    cb = base[rank, 0:1, :]
    sb = base[rank, 1:2, :]
    ctab[0:B, :] = cb * tab[0] - sb * tab[1]
    stab[0:B, :] = sb * tab[0] + cb * tab[1]
    ctab[B:B + PAD, :] = jnp.broadcast_to(base[M, 0:1, :], (PAD, HEAD))
    stab[B:B + PAD, :] = jnp.broadcast_to(base[M, 1:2, :], (PAD, HEAD))

    for c in range(1, NC):
        own_part(c)

    for d in range(1, T):
        src = lax.rem(me + T - d, T)
        pltpu.make_async_remote_copy(
            src_ref=tok_hbm, dst_ref=tokbuf.at[src], send_sem=tps.at[1, d],
            recv_sem=tpr.at[1, d], device_id={"tp": src}, device_id_type=MESH).wait_recv()
        pltpu.make_async_remote_copy(
            src_ref=x_hbm, dst_ref=xbuf.at[src, pl.ds(0, B)], send_sem=tps.at[0, d],
            recv_sem=tpr.at[0, d], device_id={"tp": src}, device_id_type=MESH).wait_recv()
        widen(src)

    def rotated(u):
        return u * ctab[...] + pltpu.roll(u, HEAD // 2, 1) * stab[...]

    def rest(m, c, total):
        for d in range(1, T):
            wcopy(m, c, d).wait()
            part = dot(xbuf[lax.rem(me + d, T)], wbuf[m, c, d])
            total = part if total is None else total + part
        return total

    steps = (lax.broadcasted_iota(jnp.int32, (B, HEAD), 0) + 1).astype(F32)

    def block_decay(c, power):
        rows = [jnp.exp(jnp.full((R, HEAD), -power * B * rate[c * hc + h], F32)) for h in range(hc)]
        return jnp.concatenate(rows, axis=0)

    def phase_kv(c):
        kk = rest(0, c, acc[0, c])
        vv = rest(1, c, acc[1, c])
        states = []
        for hh in range(hc):
            h = c * hc + hh
            cols = slice(hh * HEAD, (hh + 1) * HEAD)
            kr = rotated(kk[:, cols])
            tokk[h:h + 1, :] = kr[B:B + 1]
            krb = kr[:B].astype(BF)
            kbuf[h] = krb
            v = vv[:, cols]
            tokv[h:h + 1, :] = v[B:B + 1]
            vb = (v[:B] * jnp.exp(steps * rate[h])).astype(BF)
            vbuf[h] = vb
            st = lax.dot_general(krb, vb, (((0,), (0,)), ((), ())), preferred_element_type=F32)
            states.append(st * jnp.exp(jnp.full((HEAD, HEAD), -B * rate[h], F32)))
        for i in range(G):
            for zz in range(Z):
                lo = (zz * G + i) * R
                send1[c, i, zz] = jnp.concatenate([s[lo:lo + R] for s in states], axis=0).astype(BF)
        recv1[c, j] = send1[c, j]
        for d in range(1, G):
            i = lax.rem(j + d, G)
            cp = pltpu.make_async_remote_copy(
                src_ref=send1.at[c, i], dst_ref=recv1.at[c, j], send_sem=s1s.at[c, d],
                recv_sem=s1r.at[c, d], device_id={"sp": z * G + i}, device_id_type=MESH)
            cp.start()
            sends.append(cp)

    def full2(c, s, t):
        return pltpu.make_async_remote_copy(
            src_ref=recv2.at[c, s], dst_ref=recv2.at[c, s], send_sem=s2s.at[c, t],
            recv_sem=s2r.at[c, s], device_id={"sp": t * G + j}, device_id_type=MESH)

    def part2(c, s, t):
        return pltpu.make_async_remote_copy(
            src_ref=recv2.at[c, s, t], dst_ref=recv2.at[c, s, t], send_sem=s2s.at[c, t],
            recv_sem=s2r.at[c, s], device_id={"sp": t * G + j}, device_id_type=MESH)

    def phase_plane(c):
        for d in range(1, G):
            i = lax.rem(j + G - d, G)
            pltpu.make_async_remote_copy(
                src_ref=send1.at[c, i], dst_ref=recv1.at[c, i], send_sem=s1s.at[c, d],
                recv_sem=s1r.at[c, d], device_id={"sp": z * G + i}, device_id_type=MESH).wait_recv()
        gb = block_decay(c, 1)[None]
        run = jnp.zeros((Z, hc * R, HEAD), F32)
        for i in range(G):
            pre[c, i] = run
            run = run * gb + recv1[c, i].astype(F32)
        recv2[c, z] = run.astype(BF)
        for t in range(Z):
            @pl.when(t > z)
            def _():
                full2(c, z, t).start()

            @pl.when(t < z)
            def _():
                part2(c, z, t).start()

    def phase_chain(c):
        gz = block_decay(c, G)
        pacc[...] = jnp.zeros((Z, hc * R, HEAD), F32)
        for s in range(Z):
            @pl.when(s < z)
            def _():
                full2(c, s, z).wait_recv()
                pacc[...] = pacc[...] * gz[None] + recv2[c, s].astype(F32)
        run = pacc[...]
        gb = block_decay(c, 1)[None]
        for i in range(G):
            send3[c, i] = (run + pre[c, i]).astype(BF)
            run = run * gb
        recv3[c, j] = send3[c, j]
        for d in range(1, G):
            i = lax.rem(j + d, G)
            cp = pltpu.make_async_remote_copy(
                src_ref=send3.at[c, i], dst_ref=recv3.at[c, j], send_sem=s3s.at[c, d],
                recv_sem=s3r.at[c, d], device_id={"sp": z * G + i}, device_id_type=MESH)
            cp.start()
            sends.append(cp)

    def phase_final(c):
        gz = block_decay(c, G)
        run = jnp.zeros((hc * R, HEAD), F32)
        for s in range(Z):
            @pl.when(s > z)
            def _():
                part2(c, s, z).wait_recv()
            run = run * gz + recv2[c, s, z].astype(F32)
        fin[c * hc * R:(c + 1) * hc * R, :] = run
        for hh in range(hc):
            cache[c * hc + hh] = run[hh * R:(hh + 1) * R].astype(BF)

    half = B // 2
    causal = (lax.broadcasted_iota(jnp.int32, (half, half), 0)
              >= lax.broadcasted_iota(jnp.int32, (half, half), 1))

    def phase_q(c):
        wcopy(2, c, 0).wait()
        qq = rest(2, c, dot(xbuf[me], wbuf[2, c, 0]))
        for hh in range(hc):
            h = c * hc + hh
            qr = rotated(qq[:, hh * HEAD:(hh + 1) * HEAD])
            tokq[h:h + 1, :] = qr[B:B + 1]
            qb = qr[:B].astype(BF)
            qbuf[h] = qb
            for t in range(2):
                rows = qb[t * half:(t + 1) * half]
                out = None
                for s in range(t + 1):
                    ks = kbuf[h, s * half:(s + 1) * half, :]
                    sc = lax.dot_general(rows, ks, (((1,), (1,)), ((), ())), preferred_element_type=F32)
                    if s == t:
                        sc = jnp.where(causal, sc, 0.0)
                    part = dot(sc.astype(BF), vbuf[h, s * half:(s + 1) * half, :])
                    out = part if out is None else out + part
                intra[h, t * half:(t + 1) * half, :] = out

    def phase_tail(c):
        for d in range(1, G):
            i = lax.rem(j + G - d, G)
            pltpu.make_async_remote_copy(
                src_ref=send3.at[c, i], dst_ref=recv3.at[c, i], send_sem=s3s.at[c, d],
                recv_sem=s3r.at[c, d], device_id={"sp": z * G + i}, device_id_type=MESH).wait_recv()
        pieces = [[recv3[c, i, zz].astype(F32) for i in range(G)] for zz in range(Z)]
        for hh in range(hc):
            h = c * hc + hh
            inc = jnp.concatenate(
                [pieces[zz][i][hh * R:(hh + 1) * R] for zz in range(Z) for i in range(G)], axis=0)
            o = intra[h] + dot(qbuf[h], inc.astype(BF))
            o = o * (jnp.exp(steps * -rate[h]) * HEAD ** -0.5)
            res = head_norm(o, gain[:, h * HEAD:(h + 1) * HEAD])
            obuf[c, :, hh * HEAD:(hh + 1) * HEAD] = res.astype(BF)
        pltpu.make_async_copy(obuf.at[c], mixed.at[:, pl.ds(c * W, W)], o_sem.at[c]).start()

    def read_send():
        tq = tokq[...].astype(BF).astype(F32)
        n = H * R
        pick = (lax.broadcasted_iota(jnp.int32, (HEAD, n), 0)
                == rank * R + lax.broadcasted_iota(jnp.int32, (HEAD, n), 1) % R)
        sel = dot(tq, pick.astype(F32))
        own = (lax.broadcasted_iota(jnp.int32, (H, n), 0)
               == lax.broadcasted_iota(jnp.int32, (H, n), 1) // R)
        sel = jnp.where(own, sel, 0.0)
        rdbuf[rank] = jnp.dot(sel, fin[...], preferred_element_type=F32, precision=lax.Precision.HIGHEST)
        for d in range(1, M):
            peer = lax.rem(rank + d, M)
            cp = pltpu.make_async_remote_copy(
                src_ref=rdbuf.at[rank], dst_ref=rdbuf.at[rank], send_sem=rds.at[d],
                recv_sem=rdr.at[d], device_id={"sp": peer}, device_id_type=MESH)
            cp.start()
            sends.append(cp)

    def read_finish():
        for d in range(1, M):
            src = lax.rem(rank + M - d, M)
            pltpu.make_async_remote_copy(
                src_ref=rdbuf.at[src], dst_ref=rdbuf.at[src], send_sem=rds.at[d],
                recv_sem=rdr.at[d], device_id={"sp": src}, device_id_type=MESH).wait_recv()
        total = jnp.sum(rdbuf[...], axis=0)
        scale = HEAD ** -0.5
        tq = tokq[...].astype(BF).astype(F32)
        tk = tokk[...].astype(BF).astype(F32)
        score = jnp.sum(tq * tk, axis=-1, keepdims=True) * scale
        base_part = score * tokv[...].astype(BF).astype(F32)
        for h in range(H):
            g = jnp.exp(jnp.full((1, HEAD), -rate[h], F32)) * scale
            o = g * total[h:h + 1] + base_part[h:h + 1]
            read_out[:, h * HEAD:(h + 1) * HEAD] = head_norm(o, gain[:, h * HEAD:(h + 1) * HEAD]).astype(BF)

    work = [functools.partial(phase_kv, c) for c in range(NC)]
    work += [functools.partial(phase_q, c) for c in range(NC)]
    plane_at, chain_at = 2, 5
    planes = 0
    chains = 0
    for n, step in enumerate(work):
        step()
        if n >= plane_at and planes < NC and planes <= n:
            phase_plane(planes)
            planes += 1
        if n >= chain_at and chains < planes:
            phase_chain(chains)
            chains += 1
    while planes < NC:
        phase_plane(planes)
        planes += 1
    while chains < NC:
        phase_chain(chains)
        chains += 1
    for c in range(NC):
        phase_final(c)
    read_send()
    for c in range(NC):
        phase_tail(c)
    read_finish()
    for cp in sends:
        cp.wait_send()
    for c in range(NC):
        for t in range(Z):
            @pl.when(t > z)
            def _():
                full2(c, z, t).wait_send()

            @pl.when(t < z)
            def _():
                part2(c, z, t).wait_send()
        pltpu.make_async_copy(obuf.at[c], mixed.at[:, pl.ds(c * W, W)], o_sem.at[c]).wait()


def per_device(prompt, new_token, w_query, w_key, w_value, decay_rate, norm_gain):
    _, B, F = prompt.shape
    D = w_query.shape[0]
    H = w_query.shape[1] // HEAD
    M = lax.axis_size("sp")
    T = lax.axis_size("tp")
    G = split(M)
    Z = M // G
    R = HEAD // M
    hc = 2 if H % 2 == 0 else 1
    NC = H // hc
    W = hc * HEAD
    inverse = rope_base ** (-np.arange(0, HEAD, 2, dtype=np.float64) / HEAD)
    sign = np.concatenate([-np.ones(HEAD // 2), np.ones(HEAD // 2)])

    def pair(positions):
        angles = np.concatenate([positions[:, None] * inverse[None]] * 2, axis=1)
        return np.cos(angles), np.sin(angles) * sign[None]

    tab = np.stack(pair(np.arange(B, dtype=np.float64))).astype(np.float32)
    base = np.stack(pair(np.arange(M + 1, dtype=np.float64) * B), axis=1).astype(np.float32)
    any_ = pl.BlockSpec(memory_space=pltpu.HBM)
    vm = pl.BlockSpec(memory_space=pltpu.VMEM)
    sm = pl.BlockSpec(memory_space=pltpu.SMEM)
    V = pltpu.VMEM
    DMA = pltpu.SemaphoreType.DMA
    cfg = (M, G, Z, T, B, F, H, hc, R)
    mixed, cache, new_read = pl.pallas_call(
        functools.partial(kernel, cfg),
        out_shape=(
            jax.ShapeDtypeStruct((B, H * HEAD), BF),
            jax.ShapeDtypeStruct((H, R, HEAD), BF),
            jax.ShapeDtypeStruct((1, H * HEAD), BF),
        ),
        in_specs=[any_, any_, any_, any_, any_, sm, vm, any_, vm],
        out_specs=(any_, vm, vm),
        scratch_shapes=[
            V((T, B + PAD, F), BF),
            V((T, 1, F), BF),
            V((3, NC, T, F, W), BF),
            V((2, NC, B + PAD, W), F32),
            V((2, B, HEAD), F32),
            V((B + PAD, HEAD), F32),
            V((B + PAD, HEAD), F32),
            V((H, B, HEAD), BF),
            V((H, B, HEAD), BF),
            V((H, B, HEAD), BF),
            V((H, B, HEAD), F32),
            V((NC, B, W), BF),
            V((NC, G, Z, hc * R, HEAD), BF),
            V((NC, G, Z, hc * R, HEAD), BF),
            V((NC, G, Z, hc * R, HEAD), F32),
            V((NC, Z, Z, hc * R, HEAD), BF),
            V((NC, G, Z, hc * R, HEAD), BF),
            V((NC, G, Z, hc * R, HEAD), BF),
            V((Z, hc * R, HEAD), F32),
            V((H * R, HEAD), F32),
            V((H, HEAD), F32),
            V((H, HEAD), F32),
            V((H, HEAD), F32),
            V((M, H, HEAD), F32),
            DMA((3, NC, T)),
            DMA((3,)),
            DMA((2, T)),
            DMA((2, T)),
            DMA((NC, G)),
            DMA((NC, G)),
            DMA((NC, Z)),
            DMA((NC, Z)),
            DMA((NC, G)),
            DMA((NC, G)),
            DMA((M,)),
            DMA((M,)),
            DMA((NC,)),
        ],
        compiler_params=pltpu.CompilerParams(
            collective_id=0, has_side_effects=True, vmem_limit_bytes=60 * 1024 * 1024),
    )(prompt.reshape(B, F), new_token, w_query, w_key, w_value, decay_rate,
      norm_gain.reshape(1, H * HEAD), jnp.asarray(tab), jnp.asarray(base))
    return (mixed[None], cache[None], new_read)


def solution(mesh):
    in_specs = (
        P(None, "sp", "tp"),
        P(None, "tp"),
        P(None, "tp"),
        P(None, "tp"),
        P(None, "tp"),
        P("tp"),
        P("tp"),
    )
    out_specs = (P(None, "sp", "tp"), P(None, "tp", "sp", None), P(None, "tp"))
    return jax.shard_map(
        per_device, mesh=mesh, in_specs=in_specs, out_specs=out_specs, check_vma=False
    )
```

time: 132 us -> 45.1 us (0.34)
  Pallas kernels: 0 us -> 39.3 us
  blocking collectives: 39.2 us -> 0 us
  matrix products: 24.1 us -> 0 us
  waiting for transfers between devices: 21.4 us -> 0 us
  other arithmetic: 14.4 us -> 0 us
  between operations: 14.3 us -> 0.64 us
  starting transfers between devices: 10.4 us -> 0 us
  local copies, waits for them, and re-layouts: 7.52 us -> 4.85 us
    pallas_call x0 -> x1, Pallas kernels: none -> 39.3 us  [per_device(): pl.pallas_call(functools.partial(kernel, cfg), out_shape=(jax.ShapeDtypeS...]
    psum x1 -> x0, blocking collectives: 39.2 us -> none  [per_device(): read_sum = lax.psum(partial_value, 'sp')]
    dot_general x9 -> x0, matrix products: 24.1 us -> none  [the longest x3 10.2 us: per_device(): jnp.dot(shard_piece, weight, preferred_element_type=jnp.float32)]
    all_to_all x2 -> x0, waiting for transfers between devices: 10.8 us -> none  [the longest x1 6.98 us: per_device(): lax.all_to_all(prefix.astype(jnp.bfloat16), 'sp', split_axis=0, concat_ax...]
    all_gather x1 -> x0, waiting for transfers between devices: 10.7 us -> none  [per_device(): shard_piece = lax.all_gather(token_rows, 'tp', axis=1, tiled=True)]
    all_to_all x2 -> x0, starting transfers between devices: 10.3 us -> none  [the longest x1 6.79 us: per_device(): lax.all_to_all(local_state[None], 'sp', split_axis=3, concat_axis=0, tile...]
    concatenate x3 -> x0, other arithmetic: 5.22 us -> none  [the longest x2 2.89 us: rotate(): jnp.concatenate([first_half * cosine - second_half * sine_part, first_hal...]
    convert_element_type x8 -> x0, other arithmetic: 4.97 us -> none  [the longest x1 3.18 us: per_device(): (rotate(queries.astype(jnp.float32), positions) * HEAD ** (-0.5)).astype(...]
  transfers between devices with their start and end apart: 3 -> 0, of which waited for: 3 -> 0; matrix products, arithmetic and copies ran while one was open for 12% -> 0% of each run, Pallas kernels for 0% -> 0%
where the time goes in v1:
time: 45.1 us; the launch traced here: 44.8 us
  Pallas kernels  39.3 us (87%)
  local copies, waits for them, and re-layouts  4.85 us (11%)
  between operations  0.64 us (1%)
    pallas_call x1, Pallas kernels, per_device(): pl.pallas_call(functools.partial(kernel, cfg), out_shape=(jax.ShapeDtypeS...  39.3 us
    unnamed x3, local copies, waits for them, and re-layouts  4.85 us

profile of v1, /device:TPU:0, one launch (start us, length us, event | category | flops | bytes accessed | tf_op | source)
XLA Modules:
  0.0 44.8 jit_solution(12046079273751028169)
XLA Ops:
  0.6 39.3 %shard_map.112 = (bf16[512,1024]{1,0:T(8,128)(2,1)}, bf16[8,8,128]{2,1,0:T(8,128)(2,1)}, bf16[1,1024]{1,0:T(2,128)(2,1)}) custom-call(bf16[512,1024]{1,0:T(8,128)(2,1)} %bitcast.4, bf16[1,1024]{1,0:T(2,128)(2,1)} %tok_hbm.1, bf16[2048,1024]{1,0:T(8,128)(2,1)} %wq.1, bf16[2048,1024]{1,0:T(8,128)(2,1)} %wk.1, bf16[2048,1024]{1,0:T(8,128)(2,1)} %wv.1, f32[8]{0:T(128)} %rate.1, ...), custom_call_target="tpu_custom_call" | custom-call | tf_op jit(solution)/shard_map/pallas_call | solution.py:386
  40.0 2.3 %copy.15 = bf16[1,512,1024]{2,1,0:T(8,128)(2,1)} copy(bf16[1,512,1024]{2,1,0:T(8,128)(2,1)} %bitcast.5) | data formatting | bytes 2097152
  42.2 1.3 %copy.16 = bf16[1,8,8,128]{3,2,1,0:T(8,128)(2,1)} copy(bf16[1,8,8,128]{3,2,1,0:T(8,128)(2,1)} %bitcast.6) | data formatting | bytes 32768
  43.6 1.3 %copy.17 = bf16[1,1024]{1,0:T(2,128)(2,1)} copy(bf16[1,1024]{1,0:T(2,128)(2,1)} %get-tuple-element.14) | data formatting | bytes 4096
